TPU v7x, 32 devices: a whole 2x2x4 slice. The times are simulated.
32 devices in a mesh: sp: 8 (over z, x), tp: 4 (over y, core).
Axes of the slice: x: 2, y: 2, z: 4, core: 2. Of those that a mesh axis runs over, the one named last changes fastest.
Arguments:
- latent: bfloat16 [9216, 2048], P(('sp', 'tp')), may hold values from -0.6 to 0.6
- context: bfloat16 [32, 2048], P(('sp', 'tp')), may hold values from -6 to 6
- condition: float32 [2048], P('sp'), may hold values from -6 to 6
- context_condition: float32 [2048], P('sp'), may hold values from -6 to 6
- modulation_weight: bfloat16 [2048, 6144], P('sp', 'tp'), may hold values from -0.1875 to 0.1875
- norm_gain: float32 [2048], replicated, may hold values from 0.1 to 1.9
- query_weight: bfloat16 [2048, 1024], replicated
- key_weight: bfloat16 [2048, 256], replicated
- value_weight: bfloat16 [2048, 256], replicated, may hold values from -0.125 to 0.125
- output_weight: bfloat16 [1024, 2048], replicated, may hold values from -0.1875 to 0.1875
- query_gain: float32 [128], replicated, may hold values from 0.5 to 6
- key_gain: float32 [128], replicated, may hold values from 0.5 to 6
- sink_logit: float32 [8], replicated, may hold values from 1 to 5
Outputs:
- updated: bfloat16 [9216, 2048], P(('sp', 'tp'))
All inputs are finite; a program needn't handle non-finite values.
Results may differ from a plain program's by a relative error of at most 0.006.
The roundings to bfloat16 on the way count: a program that leaves them out, or rounds other values in their place, can miss the bound.
Values may be sent and summed in bfloat16 or wider, within the bound.
A program may use at most 64 MiB of HBM per device.

v0:
```python
import jax
import jax.numpy as jnp
from jax import lax
from jax.sharding import PartitionSpec as P

WINDOW = 128
GRID_W = 64


EPS = 1e-06
ROPE_BASE = 10000.0
FAR_LOGIT = -1e30


def with_halo(array, sides, width):
    for axis, dim in sides:
        size, length = (lax.axis_size(axis), array.shape[dim])
        up = [(i, (i + 1) % size) for i in range(size - 1)]
        down = [(j, i) for i, j in up]
        last = lax.slice_in_dim(array, length - width, length, axis=dim)
        first = lax.slice_in_dim(array, 0, width, axis=dim)
        before = lax.ppermute(last, axis, up)
        after = lax.ppermute(first, axis, down)
        array = jnp.concatenate([before, array, after], axis=dim)
    return array


def rms_rows(values_in):
    return values_in * lax.rsqrt(jnp.mean(values_in * values_in, axis=-1, keepdims=True) + EPS)


def turn_halves(halves_in):
    former, latter = jnp.split(halves_in, 2, axis=-1)
    return jnp.concatenate([-latter, former], axis=-1)


def rotary(values_in, positions):
    quarter = values_in.shape[-1] // 4
    inverse = jnp.power(ROPE_BASE, -jnp.arange(quarter, dtype=jnp.float32) / quarter)
    by_rows = (positions // GRID_W).astype(jnp.float32)[:, None] * inverse
    by_cols = (positions % GRID_W).astype(jnp.float32)[:, None] * inverse
    angles = jnp.concatenate([by_rows, by_rows, by_cols, by_cols], axis=-1)[:, None, :]
    row_half, col_half = jnp.split(values_in, 2, axis=-1)
    turned = jnp.concatenate([turn_halves(row_half), turn_halves(col_half)], axis=-1)
    return values_in * jnp.cos(angles) + turned * jnp.sin(angles)


def head_norm(flat, gain):
    per_head = flat.reshape(flat.shape[0], flat.shape[1] // gain.shape[0], gain.shape[0])
    return rms_rows(per_head) * gain


def modulated(tokens_in, norm_gain, shift, scale):
    values_in = tokens_in.astype(jnp.float32)
    return (rms_rows(values_in) * norm_gain * (1.0 + scale) + shift).astype(jnp.bfloat16)


def key_value_rows(hidden_rows, positions, key_weight, value_weight, key_gain):
    row_count = hidden_rows.shape[0]
    kv_width = key_weight.shape[1]
    keys = (
        rotary(
            head_norm(
                jnp.dot(hidden_rows, key_weight, preferred_element_type=jnp.float32), key_gain
            ),
            positions,
        )
        .astype(jnp.bfloat16)
        .reshape(row_count, kv_width)
    )
    values = jnp.dot(hidden_rows, value_weight, preferred_element_type=jnp.float32).astype(
        jnp.bfloat16
    )
    return jnp.stack([keys, values])


def attend(queries, keys, values, ctx_keys, ctx_values, sink_logit, allowed, head_size):
    row_count = queries.shape[0]
    kv_count = keys.shape[1] // head_size
    group = queries.shape[1] // keys.shape[1]
    score_scale = head_size ** (-0.5)
    grouped = queries.reshape(row_count, kv_count, group, head_size)
    near_keys = keys.reshape(keys.shape[0], kv_count, head_size)
    near_values = values.reshape(values.shape[0], kv_count, head_size)
    far_keys = ctx_keys.reshape(ctx_keys.shape[0], kv_count, head_size)
    far_values = ctx_values.reshape(ctx_values.shape[0], kv_count, head_size)
    near_scores = (
        jnp.einsum("rhgd,khd->hgrk", grouped, near_keys, preferred_element_type=jnp.float32)
        * score_scale
    )
    near_scores = jnp.where(allowed, near_scores, FAR_LOGIT)
    ctx_scores = (
        jnp.einsum("rhgd,khd->hgrk", grouped, far_keys, preferred_element_type=jnp.float32)
        * score_scale
    )
    sink_part = sink_logit.reshape(kv_count, group)[:, :, None, None]
    row_max = jnp.maximum(
        jnp.maximum(
            jnp.max(near_scores, axis=-1, keepdims=True),
            jnp.max(ctx_scores, axis=-1, keepdims=True),
        ),
        sink_part,
    )
    near_exp = jnp.exp(near_scores - row_max)
    ctx_exp = jnp.exp(ctx_scores - row_max)
    denominator = (
        jnp.sum(near_exp, axis=-1, keepdims=True)
        + jnp.sum(ctx_exp, axis=-1, keepdims=True)
        + jnp.exp(sink_part - row_max)
    )
    near_probs = (near_exp / denominator).astype(jnp.bfloat16)
    ctx_probs = (ctx_exp / denominator).astype(jnp.bfloat16)
    mixed = jnp.einsum(
        "hgrk,khd->rhgd", near_probs, near_values, preferred_element_type=jnp.float32
    ) + jnp.einsum("hgrk,khd->rhgd", ctx_probs, far_values, preferred_element_type=jnp.float32)
    return mixed.astype(jnp.bfloat16).reshape(row_count, queries.shape[1])


def local(
    latent,
    context,
    condition,
    context_condition,
    modulation_weight,
    norm_gain,
    query_weight,
    key_weight,
    value_weight,
    output_weight,
    query_gain,
    key_gain,
    sink_logit,
):
    model_width = latent.shape[1]
    head_size = query_gain.shape[0]
    kv_width = key_weight.shape[1]
    query_width = query_weight.shape[1]
    activations = jax.nn.silu(jnp.stack([condition, context_condition])).astype(jnp.bfloat16)
    partial_value = jnp.dot(activations, modulation_weight, preferred_element_type=jnp.float32)
    summed = lax.psum(partial_value, "sp")
    modulation = lax.all_gather(summed, "tp", axis=1, tiled=True)
    hidden = modulated(
        latent, norm_gain, modulation[0, :model_width], modulation[0, model_width : 2 * model_width]
    )
    ctx_hidden = modulated(
        context,
        norm_gain,
        modulation[1, :model_width],
        modulation[1, model_width : 2 * model_width],
    )
    gate = modulation[0, 2 * model_width :]
    row_count = latent.shape[0]
    row_start = lax.axis_index(("sp", "tp")) * row_count
    total_rows = row_count * lax.axis_size(("sp", "tp"))
    positions = row_start + jnp.arange(row_count, dtype=jnp.int32)
    queries = (
        rotary(
            head_norm(
                jnp.dot(hidden, query_weight, preferred_element_type=jnp.float32), query_gain
            ),
            positions,
        )
        .astype(jnp.bfloat16)
        .reshape(row_count, query_width)
    )
    local_both = key_value_rows(hidden, positions, key_weight, value_weight, key_gain)
    band = with_halo(local_both, ((("sp", "tp"), 1),), WINDOW)
    ctx_piece = lax.all_gather(ctx_hidden, ("sp", "tp"), axis=0, tiled=True)
    piece_rows = ctx_piece.shape[0]
    projected = head_norm(
        jnp.dot(ctx_piece, key_weight, preferred_element_type=jnp.float32), key_gain
    )
    projected = projected.astype(jnp.bfloat16).reshape(piece_rows, kv_width)
    value_rows = jnp.dot(ctx_piece, value_weight, preferred_element_type=jnp.float32).astype(
        jnp.bfloat16
    )
    ctx_both = jnp.concatenate([projected, value_rows], axis=1)
    key_pos = row_start - WINDOW + jnp.arange(row_count + 2 * WINDOW, dtype=jnp.int32)
    allowed = (
        (jnp.abs(key_pos[None, :] - positions[:, None]) <= WINDOW)
        & (key_pos[None, :] >= 0)
        & (key_pos[None, :] < total_rows)
    )
    mixed = attend(
        queries,
        band[0],
        band[1],
        ctx_both[:, :kv_width],
        ctx_both[:, kv_width:],
        sink_logit,
        allowed,
        head_size,
    )
    update = jnp.dot(mixed, output_weight, preferred_element_type=jnp.float32)
    return (latent.astype(jnp.float32) + gate * update).astype(jnp.bfloat16)


def solution(mesh):
    placed = (
        P(("sp", "tp"), None),
        P(("sp", "tp"), None),
        P("sp"),
        P("sp"),
        P("sp", "tp"),
        P(),
        P(),
        P(),
        P(),
        P(),
        P(),
        P(),
        P(),
    )
    return jax.shard_map(
        local, mesh=mesh, in_specs=placed, out_specs=P(("sp", "tp"), None), check_vma=False
    )
```

profile of v0, /device:TPU:0, one launch (start us, length us, event | category | flops | bytes accessed | tf_op | source)
XLA Modules:
  0.0 136.5 jit_solution(12055852137158894293)
XLA Ops:
  0.0 1.5 %multiply_reduce_fusion.3 = f32[]{:T(128)} fusion(bf16[1,2048]{1,0:T(2,128)(2,1)} %param.14), kind=kLoop, calls=%fused_computation.85 | loop fusion | flops 6143 | bytes 4100 | tf_op jit(solution)/shard_map/reduce_sum | solution.py:29
  2.2 0.7 broadcast_bitcast_fusion
  2.9 1.6 %fusion.4 = f32[288]{0:T(512)S(1)} fusion(bf16[288,2048]{1,0:T(8,128)(2,1)} %param.13), kind=kLoop, calls=%fused_computation.11 | loop fusion | flops 1769184 | bytes 1180800 | tf_op jit(solution)/shard_map/reduce_sum | solution.py:29
  4.5 1.4 %fusion.49 = f32[2,1536]{1,0:T(2,128)S(1)} fusion(bf16[256,1536]{1,0:T(8,128)(2,1)} %param.17, f32[1,256]{1,0:T(1,128)} %bitcast.97, f32[1,256]{1,0:T(1,128)} %bitcast.98), kind=kOutput, calls=%fused_computation.105 | convolution fusion | flops 1575936 | bytes 800768 | tf_op jit(solution)/shard_map/dot_general | solution.py:139
  5.9 38.9 %psum.7 = f32[2,1536]{1,0:T(2,128)S(1)} all-reduce(f32[2,1536]{1,0:T(2,128)S(1)} %fusion.49), channel_id=1, replica_groups=mesh['sp'=8,'tp'=4] {'sp'}, use_global_device_ids=true, to_apply=%region_0.1 | all-reduce | flops 3072 | bytes 24576 | tf_op jit(solution)/shard_map/psum | solution.py:140
  44.7 5.2 %all_gather.6 = f32[2,6144]{1,0:T(2,128)S(1)} all-gather(f32[2,1536]{1,0:T(2,128)S(1)} %psum.7), channel_id=1, replica_groups=mesh['sp'=8,'tp'=4] {'tp'}, dimensions={1}, use_global_device_ids=true | all-gather | bytes 61440 | tf_op jit(solution)/shard_map/all_gather | solution.py:141
  49.9 0.6 fusion.62
  50.6 0.6 fusion.16
  51.2 0.6 copy-done.9
  51.8 0.6 fusion.59
  52.4 0.2 reshape.279
  52.6 0.4 multiply_reduce_fusion.1
  53.1 0.4 multiply_multiply_fusion.1
  53.5 1.0 slice_negate_fusion.3
  54.6 0.6 fusion.37
  55.3 1.0 maximum_multiply_fusion.1
  56.3 0.4 mul.272
  56.9 0.7 pad_maximum_fusion.3
  57.6 2.9 %collective-permute-start = (bf16[2,128,256]{2,1,0:T(8,128)(2,1)}, bf16[2,128,256]{2,1,0:T(8,128)(2,1)}, u32[]{:S(2)}, u32[]{:S(2)}) collective-permute-start(bf16[2,128,256]{2,1,0:T(8,128)(2,1)} %get-tuple-element.11), channel_id=1, source_target_pairs={{0,1},{1,2},{2,3},{3,4},{4,5},{5,6},{6,7},{7,8},{8,9},{9,10},{10,1... | collective-permute-start | bytes 393224 | tf_op jit(solution)/shard_map/ppermute | solution.py:22
  60.5 1.3 collective-permute-start.1
  61.8 0.6 iota_add_fusion.1
  62.4 0.6 fusion.41
  63.0 40.1 %all-gather = bf16[32,1,2048]{2,1,0:T(2,128)(2,1)S(1)} all-gather(bf16[1,1,2048]{2,1,0:T(2,128)(2,1)S(1)} %get-tuple-element.20), channel_id=1, replica_groups=mesh['sp'=8,'tp'=4] {'sp','tp'}, dimensions={0}, use_global_device_ids=true | all-gather | bytes 135168 | tf_op jit(solution)/shard_map/all_gather | solution.py:168
  103.0 0.3 convolution_convert_fusion.1
  103.3 0.3 fusion.29
  103.6 4.0 %fusion.56 = f32[288,1024]{1,0:T(8,128)S(1)} fusion(bf16[2048,1024]{1,0:T(8,128)(2,1)} %param.19, bf16[288,2048]{1,0:T(8,128)(2,1)} %param.13, f32[2048]{0:T(1024)S(1)} %bitcast.93, f32[2048]{0:T(1024)S(1)} %bitcast.96, f32[2048]{0:T(1024)S(1)} %copy-done.15, f32[288]{0:T(512)S(1)} %add_rsqrt_fusion.3), kind=kOutput, calls=%fused_computation.113 | convolution fusion | flops 1211498496 | bytes 6579328 | tf_op jit(solution)/shard_map/dot_general | solution.py:159
  107.6 1.0 copy-done.2
  108.6 1.6 %reshape.280 = f32[288,2,4,128]{3,2,1,0:T(4,128)} reshape(f32[288,1024]{1,0:T(8,128)S(1)} %fusion.56) | data formatting | bytes 2359296 | tf_op jit(solution)/shard_map/reshape | solution.py:49
  110.2 1.7 %copy.60 = f32[288,1024]{0,1:T(8,128)S(1)} copy(f32[288,1024]{1,0:T(8,128)} %copy-done.2) | data formatting | bytes 2359296 | tf_op jit(solution)/shard_map/dot_general | solution.py:159
  112.0 0.7 max.30
  112.9 0.1 multiply_reduce_fusion
  113.1 0.3 multiply_multiply_fusion
  113.5 1.4 %copy.65 = f32[288,2,4,32]{3,0,2,1:T(8,128)} copy(f32[288,2,4,32]{0,3,2,1:T(8,128)S(1)} %bitcast.82) | data formatting | bytes 589824 | tf_op jit(solution)/shard_map/concatenate | solution.py:44
  114.9 1.4 %copy.62 = f32[288,2,4,32]{3,0,2,1:T(8,128)} copy(f32[288,2,4,32]{0,3,2,1:T(8,128)S(1)} %bitcast.81) | data formatting | bytes 589824 | tf_op jit(solution)/shard_map/concatenate | solution.py:44
  116.3 1.4 %copy.64 = f32[288,2,4,32]{3,0,2,1:T(8,128)} copy(f32[288,2,4,32]{0,3,2,1:T(8,128)S(1)} %bitcast.80) | data formatting | bytes 589824 | tf_op jit(solution)/shard_map/concatenate | solution.py:44
  117.7 1.4 %copy.63 = f32[288,2,4,32]{3,0,2,1:T(8,128)} copy(f32[288,2,4,32]{0,3,2,1:T(8,128)S(1)} %bitcast.79) | data formatting | bytes 589824 | tf_op jit(solution)/shard_map/concatenate | solution.py:44
  119.2 3.7 %fusion.13 = bf16[288,2,4,128]{3,0,2,1:T(8,128)(2,1)S(1)} fusion(f32[288,2,4,32]{3,0,2,1:T(8,128)} %copy.65, f32[288,2,4,32]{3,0,2,1:T(8,128)} %copy.64, f32[288,2,4,32]{3,0,2,1:T(8,128)} %copy.63, f32[288,2,4,32]{3,0,2,1:T(8,128)} %copy.62, f32[288,2,4,128]{3,2,1,0:T(4,128)S(1)} %copy-done.1, f32[288,128]{1,0:T(8,128)S(1)} %get-tuple-element.18, ...), kind=kLoop, calls=%fused_computation.25 | loop fusion | flops 2654208 | bytes 3253760 | tf_op jit(solution)/shard_map/convert_element_type | solution.py:163
  122.8 0.4 fusion.63
  123.2 0.3 fusion.18
  123.6 1.0 pad_maximum_fusion
  124.8 1.5 %fusion.1 = (f32[2,4,288]{2,1,0:T(4,128)S(1)}, f32[2,544,288,4]{1,2,3,0:T(8,128)S(1)}) fusion(pred[288,544]{1,0:T(8,128)(4,1)S(1)} %fusion.18, bf16[288,2,4,128]{3,0,2,1:T(8,128)(2,1)S(1)} %fusion.13, bf16[544,2,128,1]{2,1,0,3:T(2,128)(2,1)S(1)} %bitcast.86), kind=kOutput, calls=%fused_computation.4 | convolution fusion | flops 324622080 | bytes 6047744 | tf_op jit(solution)/shard_map/rhgd,khd->hgrk/dot_general | solution.py:88
  126.4 2.0 %fusion = f32[2,4,288]{2,1,0:T(4,128)S(1)} fusion(f32[2,544,288,4]{1,2,3,0:T(8,128)S(1)} %get-tuple-element.26, f32[2,4,288]{2,1,0:T(4,128)S(1)} %maximum_maximum_fusion, pred[288,544]{1,0:T(8,128)(4,1)S(1)} %fusion.18), kind=kLoop, calls=%fused_computation.3 | loop fusion | flops 5011200 | bytes 5188608 | tf_op jit(solution)/shard_map/reduce_sum | solution.py:107
  128.5 1.7 %fusion.2 = f32[2,128,4,288]{1,3,2,0:T(8,128)S(1)} fusion(f32[2,544,288,4]{1,2,3,0:T(8,128)S(1)} %get-tuple-element.26, f32[2,4,288]{2,1,0:T(4,128)S(1)} %exponential_add_fusion, f32[2,4,288]{2,1,0:T(4,128)S(1)} %maximum_maximum_fusion, pred[288,544]{1,0:T(8,128)(4,1)S(1)} %fusion.18, bf16[544,2,128,1]{2,1,0,3:T(2,128)(2,1)S(1)} %bitcast.87), kind=kOutput, calls=%fused_computation.8 | convolution fusion | flops 327131136 | bytes 6646784 | tf_op jit(solution)/shard_map/hgrk,khd->rhgd/dot_general | solution.py:113
  130.2 0.4 fusion.10
  130.6 0.3 copy.70
  130.9 0.4 reshape.284
  131.4 0.5 copy-done.6
  131.9 4.6 %fusion.3 = bf16[288,2048]{1,0:T(8,128)(2,1)} fusion(bf16[288,1024]{1,0:T(8,128)(2,1)S(1)} %reshape.284, bf16[1024,2048]{1,0:T(8,128)(2,1)} %param.22, bf16[288,2048]{1,0:T(8,128)(2,1)S(1)} %copy-done.6, f32[2048]{0:T(1024)S(1)} %bitcast.90), kind=kOutput, calls=%fused_computation.10 | convolution fusion | flops 1210318848 | bytes 7151616 | tf_op jit(solution)/shard_map/dot_general | solution.py:194
  (69 shorter events, 1.4 us)
Async XLA Ops:
  0.0 50.5 %copy-start = (bf16[2048,256]{1,0:T(8,128)(2,1)S(1)}, bf16[2048,256]{1,0:T(8,128)(2,1)}, u32[]{:S(2)}) copy-start(bf16[2048,256]{1,0:T(8,128)(2,1)} %param.21) | copy-start | bytes 3145732
  0.0 49.9 %copy-start.13 = (bf16[1,2048]{1,0:T(2,128)(2,1)S(1)}, bf16[1,2048]{1,0:T(2,128)(2,1)}, u32[]{:S(2)}) copy-start(bf16[1,2048]{1,0:T(2,128)(2,1)} %param.14) | copy-start | bytes 12292
  0.0 50.5 %copy-start.5 = (bf16[288,2048]{1,0:T(8,128)(2,1)S(1)}, bf16[288,2048]{1,0:T(8,128)(2,1)}, u32[]{:S(2)}) copy-start(bf16[288,2048]{1,0:T(8,128)(2,1)} %param.13) | copy-start | bytes 3538948
  0.0 49.9 %copy-start.15 = (f32[2048]{0:T(1024)S(1)}, f32[2048]{0:T(1024)}, u32[]{:S(2)}) copy-start(f32[2048]{0:T(1024)} %param.18) | copy-start | bytes 24580
  50.5 1.2 copy-start.9
  51.8 5.1 %copy-start.11 = (bf16[1,288,256]{2,1,0:T(8,128)(2,1)}, bf16[1,288,256]{2,1,0:T(8,128)(2,1)S(1)}, u32[]{:S(2)}) copy-start(bf16[1,288,256]{2,1,0:T(8,128)(2,1)S(1)} %fusion.16) | copy-start | bytes 442372
  51.8 1.4 copy-start.20
  52.4 0.7 copy-start.7
  54.6 2.1 %copy-start.8 = (f32[288,256]{1,0:T(8,128)S(1)}, f32[288,256]{1,0:T(8,128)}, u32[]{:S(2)}) copy-start(f32[288,256]{1,0:T(8,128)} %copy-done.7) | copy-start | bytes 884740
  55.3 1.6 %copy-start.3 = (f32[288,128]{1,0:T(8,128)}, f32[288,128]{1,0:T(8,128)S(1)}, u32[]{:S(2)}) copy-start(f32[288,128]{1,0:T(8,128)S(1)} %get-tuple-element.17) | copy-start | bytes 442372
  56.9 46.5 %copy-start.10 = (bf16[2048,256]{1,0:T(8,128)(2,1)S(1)}, bf16[2048,256]{1,0:T(8,128)(2,1)}, u32[]{:S(2)}) copy-start(bf16[2048,256]{1,0:T(8,128)(2,1)} %param.20) | copy-start | bytes 3145732
  57.6 66.0 %collective-permute-start = (bf16[2,128,256]{2,1,0:T(8,128)(2,1)}, bf16[2,128,256]{2,1,0:T(8,128)(2,1)}, u32[]{:S(2)}, u32[]{:S(2)}) collective-permute-start(bf16[2,128,256]{2,1,0:T(8,128)(2,1)} %get-tuple-element.11), channel_id=1, source_target_pairs={{0,1},{1,2},{2,3},{3,4},{4,5},{5,6},{6,7},{7,8},{8,9},{9,10},{10,1... | collective-permute-start | bytes 393224 | tf_op jit(solution)/shard_map/ppermute | solution.py:22
  60.5 63.1 %collective-permute-start.1 = (bf16[2,128,256]{2,1,0:T(8,128)(2,1)}, bf16[2,128,256]{2,1,0:T(8,128)(2,1)}, u32[]{:S(2)}, u32[]{:S(2)}) collective-permute-start(bf16[2,128,256]{2,1,0:T(8,128)(2,1)} %get-tuple-element.12), channel_id=1, source_target_pairs={{1,0},{2,1},{3,2},{4,3},{5,4},{6,5},{7,6},{8,7},{9,8},{10,9},{11,1... | collective-permute-start | bytes 393224 | tf_op jit(solution)/shard_map/ppermute | solution.py:23
  107.6 1.0 copy-start.2
  110.2 1.8 %copy-start.23 = (f32[8]{0:T(128)S(1)}, f32[8]{0:T(128)}, u32[]{:S(2)}) copy-start(f32[8]{0:T(128)} %param.25) | copy-start | bytes 100
  111.9 1.1 copy-start.21
  116.3 2.8 %copy-start.1 = (f32[288,2,4,128]{3,2,1,0:T(4,128)S(1)}, f32[288,2,4,128]{3,2,1,0:T(4,128)}, u32[]{:S(2)}) copy-start(f32[288,2,4,128]{3,2,1,0:T(4,128)} %reshape.280) | copy-start | bytes 3538948
  117.7 1.4 %copy-start.4 = (f32[288,128]{1,0:T(8,128)S(1)}, f32[288,128]{1,0:T(8,128)}, u32[]{:S(2)}) copy-start(f32[288,128]{1,0:T(8,128)} %copy-done.3) | copy-start | bytes 442372
  117.7 1.4 %copy-start.22 = (f32[128]{0:T(128)S(1)}, f32[128]{0:T(128)}, u32[]{:S(2)}) copy-start(f32[128]{0:T(128)} %param.23) | copy-start | bytes 1540
  119.1 4.1 %copy-start.14 = (s32[288]{0:T(512)S(1)}, s32[288]{0:T(512)}, u32[]{:S(2)}) copy-start(s32[288]{0:T(512)} %iota_add_fusion.1) | copy-start | bytes 3460
  119.1 4.1 %copy-start.17 = (pred[544]{0:T(1024)(128)(4,1)S(1)}, pred[544]{0:T(1024)(128)(4,1)}, u32[]{:S(2)}) copy-start(pred[544]{0:T(1024)(128)(4,1)} %get-tuple-element.31) | copy-start | bytes 1636
  119.2 4.1 %copy-start.18 = (pred[544]{0:T(1024)(128)(4,1)S(1)}, pred[544]{0:T(1024)(128)(4,1)}, u32[]{:S(2)}) copy-start(pred[544]{0:T(1024)(128)(4,1)} %get-tuple-element.32) | copy-start | bytes 1636
  119.2 4.4 %copy-start.12 = (bf16[1,288,256]{2,1,0:T(8,128)(2,1)S(1)}, bf16[1,288,256]{2,1,0:T(8,128)(2,1)}, u32[]{:S(2)}) copy-start(bf16[1,288,256]{2,1,0:T(8,128)(2,1)} %copy-done.11) | copy-start | bytes 442372
  124.8 1.5 %copy-start.19 = (f32[2,4]{1,0:T(2,128)S(1)}, f32[2,4]{1,0:T(2,128)}, u32[]{:S(2)}) copy-start(f32[2,4]{1,0:T(2,128)} %max.30) | copy-start | bytes 100
  130.6 1.3 copy-start.6
  130.6 1.3 copy-start.16
where the time goes:
time: 137 us
  blocking collectives  84.1 us (61%)
  other arithmetic  17.2 us (13%)
  matrix products  15.7 us (11%)
  local copies, waits for them, and re-layouts  14.1 us (10%)
  starting transfers between devices  4.17 us (3%)
    all_gather x1, blocking collectives, local(): ctx_piece = lax.all_gather(ctx_hidden, ('sp', 'tp'), axis=0, tiled=True)  40.1 us
    psum x1, blocking collectives, local(): summed = lax.psum(partial_value, 'sp')  38.9 us
    concatenate x4, local copies, waits for them, and re-layouts, rotary(): jnp.concatenate([turn_halves(row_half), turn_halves(col_half)], axis=-1)  5.6 us
    all_gather x1, blocking collectives, local(): modulation = lax.all_gather(summed, 'tp', axis=1, tiled=True)  5.2 us
    dot_general x1, matrix products, local(): update = jnp.dot(mixed, output_weight, preferred_element_type=jnp.float32)  4.63 us
    dot_general x1, matrix products, local(): jnp.dot(hidden, query_weight, preferred_element_type=jnp.float32)  3.99 us
    reduce_sum x5, other arithmetic, rms_rows(): jnp.mean(values_in * values_in, axis=-1, keepdims=True) + EPS  3.68 us
    convert_element_type x1, other arithmetic, local(): queries = rotary(head_norm(jnp.dot(hidden, query_weight, preferred_elemen...  3.66 us
  transfers between devices with their start and end apart: 2, of which 0 were waited for; matrix products, arithmetic and copies ran while one was open for 15% of the time, Pallas kernels for 0%

commit v1 on v0

v1 whole, which is shorter than its diff:
```python
import functools
import math

import jax
import jax.numpy as jnp
from jax import lax
from jax.experimental import pallas as pl
from jax.experimental.pallas import tpu as pltpu
from jax.sharding import PartitionSpec as P

WINDOW = 128
GRID_W = 64


EPS = 1e-06
ROPE_BASE = 10000.0
FAR_LOGIT = -1e30
MESH = pl.DeviceIdType.MESH
F32 = jnp.float32
BF16 = jnp.bfloat16


def block_rows_of(rows, extra):
    sizes = [size for size in range(64, rows + 1, 16) if rows % size == 0]
    return min(sizes, key=lambda size: (-(-(size + extra) // 128), -size)) if sizes else rows


def dot(a, b):
    return jnp.dot(a, b, preferred_element_type=F32)


def kernel(
    n_sp, n_tp,
    latent_h, context_ref, cond_ref, ctx_cond_ref, mw_h, norm_gain_ref,
    wq_h, wk_h, wv_h, wo_h, q_gain_ref, k_gain_ref, sink_ref,
    out_h,
    latent_v, mw_v, wq_v, wk_v, wv_v, wo_v, out_v,
    parts, mod_all, ctx_all, ctx_flat, normed, hidden, ctx_hidden,
    cos_v, sin_v, bias_v, q_v, kv_ext, ctx_kv, mixed_v,
    load_sem, out_sem,
    part_send, part_recv, ctx_send, ctx_recv,
    mod_send, mod_recv, row_send, row_recv, halo_send, halo_recv,
):
    rows, width = latent_v.shape
    cols = mw_v.shape[1]
    head = q_gain_ref.shape[-1]
    kv_width = wk_v.shape[1]
    kv_heads = kv_width // head
    heads = wq_v.shape[1] // head
    group = heads // kv_heads
    own_ctx = context_ref.shape[0]
    n_ctx = ctx_flat.shape[0]
    sp, tp = lax.axis_index("sp"), lax.axis_index("tp")
    me = sp * n_tp + tp
    total = n_sp * n_tp
    before = lax.rem(me + total - 1, total)
    after = lax.rem(me + 1, total)

    def place(flat):
        return {"sp": lax.div(flat, n_tp), "tp": lax.rem(flat, n_tp)}

    loads = [
        pltpu.make_async_copy(src, dst, load_sem.at[i])
        for i, (src, dst) in enumerate(
            [(mw_h, mw_v), (latent_h, latent_v), (wk_h, wk_v), (wv_h, wv_v), (wq_h, wq_v), (wo_h, wo_v)]
        )
    ]
    for load in loads:
        load.start()

    barrier = pltpu.get_barrier_semaphore()
    for d in range(1, n_sp):
        pl.semaphore_signal(barrier, inc=1, device_id={"sp": lax.rem(sp + d, n_sp), "tp": tp}, device_id_type=MESH)
    for d in range(1, n_tp):
        pl.semaphore_signal(barrier, inc=1, device_id={"sp": sp, "tp": lax.rem(tp + d, n_tp)}, device_id_type=MESH)
    pl.semaphore_signal(barrier, inc=1, device_id=place(before), device_id_type=MESH)
    pl.semaphore_signal(barrier, inc=1, device_id=place(after), device_id_type=MESH)

    ctx_rows = context_ref[...].astype(F32)
    for r in range(own_ctx):
        ctx_all[tp, sp * own_ctx + r] = ctx_rows[r : r + 1]
    c0 = cond_ref[...].reshape(1, -1)
    c1 = ctx_cond_ref[...].reshape(1, -1)
    pick = lax.broadcasted_iota(jnp.int32, (8, c0.shape[1]), 0) == 0
    both = jnp.where(pick, c0, c1)
    activations = (both * jax.nn.sigmoid(both)).astype(BF16)
    loads[0].wait()
    parts[sp] = dot(activations, mw_v[...])[0:2]

    pl.semaphore_wait(barrier, n_sp + n_tp)

    part_copies, ctx_copies = [], []
    for d in range(1, n_sp):
        there = {"sp": lax.rem(sp + d, n_sp), "tp": tp}
        copy = pltpu.make_async_remote_copy(
            src_ref=parts.at[sp], dst_ref=parts.at[sp],
            send_sem=part_send.at[d], recv_sem=part_recv.at[d],
            device_id=there, device_id_type=MESH,
        )
        copy.start()
        part_copies.append(copy)
    for d in range(1, n_sp):
        there = {"sp": lax.rem(sp + d, n_sp), "tp": tp}
        mine = ctx_all.at[tp, pl.ds(sp * own_ctx, own_ctx)]
        copy = pltpu.make_async_remote_copy(
            src_ref=mine, dst_ref=mine,
            send_sem=ctx_send.at[d], recv_sem=ctx_recv.at[d],
            device_id=there, device_id_type=MESH,
        )
        copy.start()
        ctx_copies.append(copy)

    first = me * rows
    shift_bits = GRID_W.bit_length() - 1
    lane = lax.broadcasted_iota(jnp.int32, (1, head), 1)
    quarter = head // 4
    inverse = jnp.exp((lane % quarter).astype(F32) * (-math.log(ROPE_BASE) / quarter))
    pos = first + lax.broadcasted_iota(jnp.int32, (rows, head), 0)
    by_row = lax.shift_right_logical(pos, shift_bits).astype(F32)
    by_col = lax.bitwise_and(pos, GRID_W - 1).astype(F32)
    angle = jnp.where(lane < 2 * quarter, by_row, by_col) * inverse
    former = lax.rem(lane, 2 * quarter) < quarter
    cos_v[...] = jnp.cos(angle)
    sin_v[...] = jnp.where(former, -1.0, 1.0) * jnp.sin(angle)

    block = bias_v.shape[1]
    span = block + 2 * WINDOW
    for b in range(rows // block):
        qi = lax.broadcasted_iota(jnp.int32, (block, span + n_ctx), 0)
        kj = lax.broadcasted_iota(jnp.int32, (block, span + n_ctx), 1)
        kp = first + (b * block - WINDOW) + kj
        ok = (kj >= qi) & (kj <= qi + 2 * WINDOW) & (kp >= 0) & (kp < rows * total)
        bias_v[b] = jnp.where(ok | (kj >= span), 0.0, FAR_LOGIT)

    gain = norm_gain_ref[...].reshape(1, -1)
    loads[1].wait()
    step = 32

    def norm_rows(i, carry):
        at = pl.ds(pl.multiple_of(i * step, step), step)
        x = latent_v[at, :].astype(F32)
        normed[at, :] = x * lax.rsqrt(jnp.mean(x * x, axis=-1, keepdims=True) + EPS) * gain
        return carry

    lax.fori_loop(0, rows // step, norm_rows, 0)

    for copy in part_copies:
        copy.wait_recv()
    summed = parts[0]
    for i in range(1, n_sp):
        summed = summed + parts[i]
    mod_all[tp] = summed
    mod_copies, row_copies = [], []
    for d in range(1, n_tp):
        there = {"sp": sp, "tp": lax.rem(tp + d, n_tp)}
        copy = pltpu.make_async_remote_copy(
            src_ref=mod_all.at[tp], dst_ref=mod_all.at[tp],
            send_sem=mod_send.at[d], recv_sem=mod_recv.at[d],
            device_id=there, device_id_type=MESH,
        )
        copy.start()
        mod_copies.append(copy)
    for copy in ctx_copies:
        copy.wait_recv()
    for d in range(1, n_tp):
        there = {"sp": sp, "tp": lax.rem(tp + d, n_tp)}
        copy = pltpu.make_async_remote_copy(
            src_ref=ctx_all.at[tp], dst_ref=ctx_all.at[tp],
            send_sem=row_send.at[d], recv_sem=row_recv.at[d],
            device_id=there, device_id_type=MESH,
        )
        copy.start()
        row_copies.append(copy)
    loads[2].wait()
    loads[3].wait()
    for copy in mod_copies:
        copy.wait_recv()
    modulation = jnp.concatenate([mod_all[t] for t in range(n_tp)], axis=1)
    shift_0 = modulation[0:1, :width]
    scale_0 = 1.0 + modulation[0:1, width : 2 * width]
    gate_0 = modulation[0:1, 2 * width :]
    shift_1 = modulation[1:2, :width]
    scale_1 = 1.0 + modulation[1:2, width : 2 * width]

    def modulate_rows(i, carry):
        at = pl.ds(pl.multiple_of(i * step, step), step)
        hidden[at, :] = (normed[at, :] * scale_0 + shift_0).astype(BF16)
        return carry

    lax.fori_loop(0, rows // step, modulate_rows, 0)

    def head_norm(x, gain_ref):
        scale = lax.rsqrt(jnp.mean(x * x, axis=-1, keepdims=True) + EPS)
        return x * scale * gain_ref[...].reshape(1, -1)

    def rotary(x):
        turned = jnp.where(former, pltpu.roll(x, head - quarter, 1), pltpu.roll(x, quarter, 1))
        return x * cos_v[...] + turned * sin_v[...]

    keys = dot(hidden[...], wk_v[...])
    for g in range(kv_heads):
        at = slice(g * head, (g + 1) * head)
        kv_ext[WINDOW : WINDOW + rows, at] = rotary(head_norm(keys[:, at], k_gain_ref)).astype(BF16)
    kv_ext[WINDOW : WINDOW + rows, kv_width:] = dot(hidden[...], wv_v[...]).astype(BF16)

    halo = [
        pltpu.make_async_remote_copy(
            src_ref=kv_ext.at[pl.ds(WINDOW, WINDOW)], dst_ref=kv_ext.at[pl.ds(WINDOW + rows, WINDOW)],
            send_sem=halo_send.at[0], recv_sem=halo_recv.at[0],
            device_id=place(before), device_id_type=MESH,
        ),
        pltpu.make_async_remote_copy(
            src_ref=kv_ext.at[pl.ds(rows, WINDOW)], dst_ref=kv_ext.at[pl.ds(0, WINDOW)],
            send_sem=halo_send.at[1], recv_sem=halo_recv.at[1],
            device_id=place(after), device_id_type=MESH,
        ),
    ]
    for copy in halo:
        copy.start()

    loads[4].wait()
    pair = 2 * head
    for c in range(heads * head // pair):
        both_heads = dot(hidden[...], wq_v[:, c * pair : (c + 1) * pair])
        for k in range(2):
            q_v[2 * c + k] = rotary(
                head_norm(both_heads[:, k * head : (k + 1) * head], q_gain_ref)
            ).astype(BF16)

    for copy in row_copies:
        copy.wait_recv()
    per = n_ctx // n_tp
    for t in range(n_tp):
        for r in range(per):
            ctx_flat[t * per + r : t * per + r + 1, :] = ctx_all[t, r]
    x = ctx_flat[...]
    x = x * lax.rsqrt(jnp.mean(x * x, axis=-1, keepdims=True) + EPS) * gain
    ctx_hidden[...] = (x * scale_1 + shift_1).astype(BF16)
    keys = dot(ctx_hidden[...], wk_v[...])
    for g in range(kv_heads):
        at = slice(g * head, (g + 1) * head)
        ctx_kv[:, at] = head_norm(keys[:, at], k_gain_ref).astype(BF16)
    ctx_kv[:, kv_width:] = dot(ctx_hidden[...], wv_v[...]).astype(BF16)

    for copy in halo:
        copy.wait_recv()

    score_scale = head ** (-0.5)
    for b in range(rows // block):
        base = b * block
        for g in range(kv_heads):
            k_at = slice(g * head, (g + 1) * head)
            v_at = slice(kv_width + g * head, kv_width + (g + 1) * head)
            k_cat = jnp.concatenate([kv_ext[base : base + span, k_at], ctx_kv[:, k_at]], axis=0)
            v_cat = jnp.concatenate([kv_ext[base : base + span, v_at], ctx_kv[:, v_at]], axis=0)
            stacked = jnp.concatenate(
                [q_v[g * group + h, base : base + block, :] for h in range(group)], axis=0
            )
            scores = lax.dot_general(
                stacked, k_cat, (((1,), (1,)), ((), ())), preferred_element_type=F32
            )
            probs = []
            for h in range(group):
                sink = sink_ref[g * group + h]
                s = scores[h * block : (h + 1) * block] * score_scale + bias_v[b]
                m = jnp.maximum(jnp.max(s, axis=-1, keepdims=True), sink)
                e = jnp.exp(s - m)
                denominator = jnp.sum(e, axis=-1, keepdims=True) + jnp.exp(sink - m)
                probs.append((e * (1.0 / denominator)).astype(BF16))
            mixed = dot(jnp.concatenate(probs, axis=0), v_cat).astype(BF16)
            for h in range(group):
                at = (g * group + h) * head
                mixed_v[base : base + block, at : at + head] = mixed[h * block : (h + 1) * block]

    loads[5].wait()
    chunk = 256
    outs = []
    for c in range(width // chunk):
        at = slice(c * chunk, (c + 1) * chunk)
        update = dot(mixed_v[...], wo_v[:, at])
        out_v[:, at] = (latent_v[:, at].astype(F32) + gate_0[:, at] * update).astype(BF16)
        view = pl.ds(c * chunk, chunk)
        copy = pltpu.make_async_copy(out_v.at[:, view], out_h.at[:, view], out_sem.at[c])
        copy.start()
        outs.append(copy)
    for copy in part_copies + ctx_copies + mod_copies + row_copies + halo:
        copy.wait_send()
    for copy in outs:
        copy.wait()


def local(n_sp, n_tp, *args):
    (latent, context, condition, context_condition, modulation_weight, norm_gain,
     query_weight, key_weight, value_weight, output_weight, query_gain, key_gain, sink_logit) = args
    rows, width = latent.shape
    cols = modulation_weight.shape[1]
    n_ctx = context.shape[0] * n_sp * n_tp
    head = query_gain.shape[0]
    kv_width = key_weight.shape[1]
    q_width = query_weight.shape[1]
    block = block_rows_of(rows, 2 * WINDOW + n_ctx)
    dma = pltpu.SemaphoreType.DMA
    hbm = pl.BlockSpec(memory_space=pl.ANY)
    vmem = pl.BlockSpec(memory_space=pltpu.VMEM)
    smem = pl.BlockSpec(memory_space=pltpu.SMEM)
    return pl.pallas_call(
        functools.partial(kernel, n_sp, n_tp),
        out_shape=jax.ShapeDtypeStruct(latent.shape, latent.dtype),
        in_specs=[hbm, vmem, vmem, vmem, hbm, vmem, hbm, hbm, hbm, hbm, vmem, vmem, smem],
        out_specs=hbm,
        scratch_shapes=[
            pltpu.VMEM(latent.shape, BF16),
            pltpu.VMEM(modulation_weight.shape, BF16),
            pltpu.VMEM(query_weight.shape, BF16),
            pltpu.VMEM(key_weight.shape, BF16),
            pltpu.VMEM(value_weight.shape, BF16),
            pltpu.VMEM(output_weight.shape, BF16),
            pltpu.VMEM(latent.shape, BF16),
            pltpu.VMEM((n_sp, 2, cols), F32),
            pltpu.VMEM((n_tp, 2, cols), F32),
            pltpu.VMEM((n_tp, n_ctx // n_tp, 1, width), F32),
            pltpu.VMEM((n_ctx, width), F32),
            pltpu.VMEM((rows, width), F32),
            pltpu.VMEM((rows, width), BF16),
            pltpu.VMEM((n_ctx, width), BF16),
            pltpu.VMEM((rows, head), F32),
            pltpu.VMEM((rows, head), F32),
            pltpu.VMEM((rows // block, block, block + 2 * WINDOW + n_ctx), F32),
            pltpu.VMEM((q_width // head, rows, head), BF16),
            pltpu.VMEM((rows + 2 * WINDOW, 2 * kv_width), BF16),
            pltpu.VMEM((n_ctx, 2 * kv_width), BF16),
            pltpu.VMEM((rows, q_width), BF16),
            dma((6,)),
            dma((width // 256,)),
            dma((n_sp,)), dma((n_sp,)), dma((n_sp,)), dma((n_sp,)),
            dma((n_tp,)), dma((n_tp,)), dma((n_tp,)), dma((n_tp,)),
            dma((2,)), dma((2,)),
        ],
        compiler_params=pltpu.CompilerParams(
            collective_id=0, has_side_effects=True, vmem_limit_bytes=60 * 1024 * 1024
        ),
        name="band_layer",
    )(*args)


def solution(mesh):
    placed = (
        P(("sp", "tp"), None),
        P(("sp", "tp"), None),
        P("sp"),
        P("sp"),
        P("sp", "tp"),
        P(),
        P(),
        P(),
        P(),
        P(),
        P(),
        P(),
        P(),
    )
    body = functools.partial(local, mesh.shape["sp"], mesh.shape["tp"])
    return jax.shard_map(
        body, mesh=mesh, in_specs=placed, out_specs=P(("sp", "tp"), None), check_vma=False
    )
```

time: 137 us -> 29.6 us (0.22)
  blocking collectives: 84.1 us -> 0 us
  Pallas kernels: 0 us -> 27 us
  other arithmetic: 17.2 us -> 0 us
  matrix products: 15.7 us -> 0 us
  local copies, waits for them, and re-layouts: 14.1 us -> 2.41 us
  starting transfers between devices: 4.17 us -> 0 us
    all_gather x2 -> x0, blocking collectives: 45.3 us -> none  [the longest x1 40.1 us: local(): ctx_piece = lax.all_gather(ctx_hidden, ('sp', 'tp'), axis=0, tiled=True)]
    psum x1 -> x0, blocking collectives: 38.9 us -> none  [local(): summed = lax.psum(partial_value, 'sp')]
    pallas_call x0 -> x1, Pallas kernels: none -> 27 us  [local(): pl.pallas_call(functools.partial(kernel, n_sp, n_tp), out_shape=jax.Shape...]
    dot_general x11 -> x0, matrix products: 15.7 us -> none  [the longest x1 4.63 us: local(): update = jnp.dot(mixed, output_weight, preferred_element_type=jnp.float32)]
    reduce_sum x7 -> x0, other arithmetic: 5.73 us -> none  [the longest x5 3.68 us: rms_rows(): jnp.mean(values_in * values_in, axis=-1, keepdims=True) + EPS]
    concatenate x4 -> x0, local copies, waits for them, and re-layouts: 5.6 us -> none  [rotary(): jnp.concatenate([turn_halves(row_half), turn_halves(col_half)], axis=-1)]
    ppermute x2 -> x0, starting transfers between devices: 4.17 us -> none  [the longest x1 2.89 us: with_halo(): before = lax.ppermute(last, axis, up)]
    convert_element_type x4 -> x0, other arithmetic: 3.85 us -> none  [the longest x1 3.66 us: local(): queries = rotary(head_norm(jnp.dot(hidden, query_weight, preferred_elemen...]
  transfers between devices with their start and end apart: 2 -> 0, of which waited for: 0 -> 0; matrix products, arithmetic and copies ran while one was open for 15% -> 0% of each run, Pallas kernels for 0% -> 0%
where the time goes in v1:
time: 29.6 us; the launch traced here: 29.4 us
  Pallas kernels  27 us (91%)
  local copies, waits for them, and re-layouts  2.41 us (8%)
    pallas_call x1, Pallas kernels, local(): pl.pallas_call(functools.partial(kernel, n_sp, n_tp), out_shape=jax.Shape...  27 us
    unnamed x1, local copies, waits for them, and re-layouts  2.41 us

profile of v1, /device:TPU:0, one launch (start us, length us, event | category | flops | bytes accessed | tf_op | source)
XLA Modules:
  0.0 29.4 jit_solution(10398577555007895783)
XLA Ops:
  0.0 27.0 %band_layer.1 = bf16[288,2048]{1,0:T(8,128)(2,1)} custom-call(bf16[288,2048]{1,0:T(8,128)(2,1)} %latent_h.1, bf16[1,2048]{1,0:T(2,128)(2,1)} %context_ref.1, f32[256]{0:T(256)} %cond_ref.1, f32[256]{0:T(256)} %ctx_cond_ref.1, bf16[256,1536]{1,0:T(8,128)(2,1)} %mw_h.1, f32[2048]{0:T(1024)} %norm_gain_ref.1, bf16[2048,1024]{1,0:T(8,128)(2,1)} %wq_h.1, ...), custom_call_target="tpu_custom_call" | custom-call | tf_op jit(solution)/shard_map/band_layer/pallas_call | solution.py:306
  27.0 2.4 %copy.15 = bf16[288,2048]{1,0:T(8,128)(2,1)} copy(bf16[288,2048]{1,0:T(8,128)(2,1)} %band_layer.1) | data formatting | bytes 2359296
